TPU v7x, 512 devices: a whole 4x4x16 slice. The times are simulated.
512 devices in a mesh: sp: 16 (over z), fs: 4 (over y), tp: 8 (over x, core).
Axes of the slice: x: 4, y: 4, z: 16, core: 2. Of those that a mesh axis runs over, the one named last changes fastest.
Arguments:
- inputs: bfloat16 [4, 4096, 4096], P('fs', 'sp', 'tp'), may hold values from -6 to 6
- norm_gain: float32 [4096], replicated, may hold values from 0.1 to 1.9
- conv_in_a: bfloat16 [4096, 1024], P(('sp', 'fs'), 'tp'), may hold values from -0.09375 to 0.09375
- conv_in_b: bfloat16 [4096, 1024], P(('sp', 'fs'), 'tp'), may hold values from -0.09375 to 0.09375
- query_w: bfloat16 [4096, 512], P(('sp', 'fs'), 'tp'), may hold values from -0.09375 to 0.09375
- key_w: bfloat16 [4096, 512], P(('sp', 'fs'), 'tp'), may hold values from -0.09375 to 0.09375
- value_w: bfloat16 [4096, 1024], P(('sp', 'fs'), 'tp'), may hold values from -0.09375 to 0.09375
- out_gate_w: bfloat16 [4096, 1024], P(('sp', 'fs'), 'tp'), may hold values from -0.09375 to 0.09375
- pointwise_w: bfloat16 [4096, 1024], P(('sp', 'fs'), 'tp'), may hold values from -0.1875 to 0.1875
- gla_out_w: bfloat16 [4096, 1024], P(('sp', 'fs'), 'tp'), may hold values from -0.1875 to 0.1875
- forget_first_factor: bfloat16 [4096, 64], replicated, may hold values from -0.09375 to 0.09375
- decay_w: bfloat16 [64, 512], replicated, may hold values from -0.75 to 0.75
- decay_bias: float32 [512], replicated, as said below
- decay_extra: float32 [4, 4096, 512], P('fs', 'sp', 'tp'), may hold values from -2.2 to 0, as said below
- conv_kernel: float32 [31, 1024], replicated, may hold values from -7 to 7
- conv_gain: float32 [1024], replicated, may hold values from 0.1 to 1.9
- head_gain: float32 [64], replicated, may hold values from 0.1 to 1.9
Outputs:
- mixed: bfloat16 [4, 4096, 4096], P('fs', 'sp', 'tp')
Inputs may be any that keep to these rules, and one draw needn't show every extreme that they name: decay_bias is positive. decay_extra is never positive.
All inputs are finite; a program needn't handle non-finite values.
Results may differ from a plain program's by a relative error of at most 0.015.
Values may be sent and summed in bfloat16 or wider, within the bound.
A program may use at most 128 MiB of HBM per device.

v0:
```python
import jax
import jax.numpy as jnp
from jax import lax
from jax.sharding import PartitionSpec as P

DK = 32
DV = 64
BLOCK = 64


def side_by_side(arrays, axis, dim, along):
    ends, at = ([], 0)
    for a in arrays[:-1]:
        at += a.shape[along]
        ends.append(at)
    both = jnp.concatenate(arrays, axis=along)
    return tuple(jnp.split(lax.all_gather(both, axis, axis=dim, tiled=True), ends, axis=along))


def from_everyone(value, axis):
    length = lax.axis_size(axis)
    return lax.all_to_all(
        jnp.broadcast_to(value[None], (length, *value.shape)), axis, 0, 0, tiled=True
    )


def in_order(tiles, dim):
    lengths = list(tiles.shape[1:])
    lengths[dim] *= tiles.shape[0]
    return jnp.moveaxis(tiles, 0, dim).reshape(lengths)


def gathered_copies(value, axis, dim):
    tiles = from_everyone(value, axis)
    return in_order(tiles, dim)


def from_behind(value, axis, by):
    length = lax.axis_size(axis)
    pairs = [(i, i + by) for i in range(length) if 0 <= i + by < length]
    return lax.ppermute(value, axis, pairs)


def over_copies(value, axis):
    everything = from_everyone(value, axis)
    return jnp.sum(everything, axis=0)


def in_one(arrays, axis):
    vector, at, outs = (jnp.concatenate([a.reshape(-1) for a in arrays]), 0, [])
    subtotal = over_copies(vector, axis)
    for a in arrays:
        outs.append(subtotal[at : at + a.size].reshape(a.shape))
        at += a.size
    return tuple(outs)


def in_blocks(value, dim, length):
    lengths = value.shape
    tiles = value.reshape(*lengths[:dim], length, lengths[dim] // length, *lengths[dim + 1 :])
    return jnp.moveaxis(tiles, dim, 0)


def sum_at_owner(value, axis, dim):
    length = lax.axis_size(axis)
    tiles = lax.all_to_all(in_blocks(value, dim, length), axis, 0, 0, tiled=True)
    return jnp.sum(tiles.astype(jnp.float32), axis=0)


def shards(
    inputs,
    norm_gain,
    conv_in_a,
    conv_in_b,
    query_w,
    key_w,
    value_w,
    out_gate_w,
    pointwise_w,
    gla_out_w,
    forget_first_factor,
    decay_w,
    decay_bias,
    decay_extra,
    conv_kernel,
    conv_gain,
    head_gain,
):
    nearer = side_by_side(
        (conv_in_a, conv_in_b, query_w, key_w, value_w, out_gate_w, pointwise_w, gla_out_w),
        "fs",
        0,
        1,
    )
    collected = side_by_side(
        (nearer[0], nearer[1], nearer[2], nearer[3], nearer[4], nearer[5], nearer[6], nearer[7]),
        "sp",
        0,
        1,
    )
    (
        conv_a_full,
        conv_b_full,
        query_full,
        key_full,
        value_full,
        gate_full,
        pointwise_full,
        gla_out_full,
    ) = collected
    tok_rows = inputs[0]
    token_count = tok_rows.shape[0]
    in_weights = (
        conv_a_full,
        conv_b_full,
        query_full,
        key_full,
        value_full,
        gate_full,
        forget_first_factor,
    )
    segment_values = gathered_copies(tok_rows, "tp", 1).astype(jnp.float32)
    scaled = (segment_values * norm_gain).astype(jnp.bfloat16)
    sums = tuple(
        (jnp.dot(scaled, weight, preferred_element_type=jnp.float32) for weight in in_weights)
    )
    sums, squares = (sums, jnp.sum(segment_values * segment_values, axis=1))
    row_scale = lax.rsqrt(squares / norm_gain.shape[0] + 1e-06)[:, None]
    conv_a, conv_b, queries, keys, values, out_gate, low_rank = [
        (running * row_scale).astype(jnp.bfloat16) for running in sums
    ]
    gated = (conv_a.astype(jnp.float32) * jax.nn.sigmoid(conv_b.astype(jnp.float32))).astype(
        jnp.bfloat16
    )
    reach = conv_kernel.shape[0] - 1
    earlier = from_behind(gated[token_count - reach :], "sp", 1)
    extended = jnp.concatenate([earlier, gated], axis=0).astype(jnp.float32)
    tp_index = lax.axis_index("tp")
    channels = gated.shape[1]
    kernel = lax.dynamic_slice_in_dim(conv_kernel, tp_index * channels, channels, 1)
    convolved = jnp.zeros((token_count, channels), jnp.float32)
    for offset in range(reach + 1):
        convolved = convolved + kernel[offset] * extended[offset : offset + token_count]
    channel_sum, channel_squares = in_one(
        (jnp.sum(convolved, axis=1), jnp.sum(convolved * convolved, axis=1)), "tp"
    )
    total_channels = conv_gain.shape[0]
    average = channel_sum / total_channels
    spread_squared_mean = channel_squares / total_channels - average * average
    gain_part = lax.dynamic_slice_in_dim(conv_gain, tp_index * channels, channels)
    normed = (
        (convolved - average[:, None]) * lax.rsqrt(spread_squared_mean + 1e-05)[:, None] * gain_part
    )
    conv_act = jax.nn.silu(normed).astype(jnp.bfloat16)
    key_width = keys.shape[1]
    head_count = key_width // DK
    decay_part = lax.dynamic_slice_in_dim(decay_w, tp_index * key_width, key_width, 1)
    bias_part = lax.dynamic_slice_in_dim(decay_bias, tp_index * key_width, key_width)
    pre_decay = jnp.dot(low_rank, decay_part, preferred_element_type=jnp.float32) + bias_part
    log_decay = jax.nn.log_sigmoid(pre_decay) / 16.0 + decay_extra[0]
    block_count = token_count // BLOCK
    highest = lax.Precision.HIGHEST

    def split_blocks(array_operand, width):
        return array_operand.reshape(block_count, BLOCK, head_count, width).transpose(0, 2, 1, 3)

    q_blocks = split_blocks(queries.astype(jnp.float32), DK) * DK ** (-0.5)
    k_blocks = split_blocks(keys.astype(jnp.float32), DK)
    v_blocks = split_blocks(values.astype(jnp.float32), DV)
    prefix_running_sum = jnp.cumsum(split_blocks(log_decay, DK), axis=2)
    causal = jnp.tril(jnp.ones((BLOCK, BLOCK), dtype=bool))
    spread = prefix_running_sum[:, :, :, None, :] - prefix_running_sum[:, :, None, :, :]
    weights_in = jnp.exp(jnp.where(causal[:, :, None], spread, -jnp.inf))
    scores = jnp.einsum("nhid,nhjd,nhijd->nhij", q_blocks, k_blocks, weights_in, precision=highest)
    inner = jnp.einsum("nhij,nhjv->nhiv", scores, v_blocks, precision=highest)
    block_total = prefix_running_sum[:, :, -1]
    block_state = jnp.einsum(
        "nhjd,nhjv->nhdv",
        k_blocks * jnp.exp(block_total[:, :, None] - prefix_running_sum),
        v_blocks,
        precision=highest,
    )

    def advance(state, block_pair):
        decay_row, added_share_term = block_pair
        return (jnp.exp(decay_row)[..., None] * state + added_share_term, state)

    local_final, local_entering = lax.scan(
        advance, jnp.zeros((head_count, DK, DV), jnp.float32), (block_total, block_state)
    )
    device_total = jnp.sum(block_total, axis=0)
    totals = lax.all_gather(device_total[None], "sp", axis=0, tiled=True)
    running_totals = jnp.cumsum(totals, axis=0)
    sp_index = lax.axis_index("sp")
    before = lax.dynamic_index_in_dim(
        running_totals, sp_index, 0, False
    ) - lax.dynamic_index_in_dim(totals, sp_index, 0, False)
    piece = lax.all_gather(local_final[None], "sp", axis=0, tiled=True)
    number = piece.shape[0]
    anchor = jnp.arange(number, dtype=jnp.int32)
    exponent = jnp.where(
        (anchor < sp_index)[:, None, None], before[None] - running_totals, -jnp.inf
    )
    entering = jnp.einsum("nhd,nhdv->hdv", jnp.exp(exponent), piece, precision=highest)
    passed = jnp.exp(jnp.cumsum(block_total, axis=0) - block_total)
    entering_blocks = passed[..., None] * entering[None] + local_entering
    outer = jnp.einsum(
        "nhid,nhdv->nhiv",
        q_blocks * jnp.exp(prefix_running_sum),
        entering_blocks,
        precision=highest,
    )
    head_output = inner + outer
    normed_heads = (
        head_output
        * lax.rsqrt(jnp.mean(head_output * head_output, axis=-1, keepdims=True) + 1e-06)
        * head_gain
    )
    gla_rows = normed_heads.transpose(0, 2, 1, 3).reshape(token_count, head_count * DV)
    gla_act = (gla_rows * jax.nn.silu(out_gate.astype(jnp.float32))).astype(jnp.bfloat16)
    contract = (((1,), (1,)), ((), ()))
    conv_term = lax.dot_general(
        pointwise_full, conv_act, contract, preferred_element_type=jnp.float32
    )
    summed = sum_at_owner(
        (
            conv_term
            + lax.dot_general(gla_out_full, gla_act, contract, preferred_element_type=jnp.float32)
        ).astype(jnp.bfloat16),
        "tp",
        0,
    )
    return (tok_rows.astype(jnp.float32) + summed.T).astype(jnp.bfloat16)[None]


def solution(mesh):
    return jax.shard_map(
        shards,
        mesh=mesh,
        in_specs=(
            P("fs", "sp", "tp"),
            P(),
            P(("sp", "fs"), "tp"),
            P(("sp", "fs"), "tp"),
            P(("sp", "fs"), "tp"),
            P(("sp", "fs"), "tp"),
            P(("sp", "fs"), "tp"),
            P(("sp", "fs"), "tp"),
            P(("sp", "fs"), "tp"),
            P(("sp", "fs"), "tp"),
            P(),
            P(),
            P(),
            P("fs", "sp", "tp"),
            P(),
            P(),
            P(),
        ),
        out_specs=P("fs", "sp", "tp"),
        check_vma=False,
    )
```

profile of v0, /device:TPU:1, one launch (start us, length us, event | category | flops | bytes accessed | tf_op | source)
XLA Modules:
  0.0 245.8 jit_solution(409942196637541957)
XLA Ops:
  7.5 12.3 %all_gather.12 = bf16[256,896]{1,0:T(8,128)(2,1)} all-gather(bf16[64,896]{1,0:T(8,128)(2,1)S(1)} %concatenate.11), channel_id=1, replica_groups=mesh['sp'=16,'fs'=4,'tp'=8] {'fs'}, dimensions={0}, use_global_device_ids=true | all-gather | bytes 573440 | tf_op jit(solution)/shard_map/all_gather | solution.py:17
  22.4 11.6 %all-to-all-start = ((bf16[8,256,512]{1,2,0:T(8,128)(2,1)}), bf16[8,256,512]{1,2,0:T(8,128)(2,1)S(1)}, u32[]{:S(2)}, u32[]{:S(2)}) async-start(bf16[8,256,512]{1,2,0:T(8,128)(2,1)} %broadcast_in_dim.45), calls=%async_computation | async-start | bytes 4194304 | tf_op jit(solution)/shard_map/all_to_all | solution.py:22
  37.8 1.9 fusion.98
  39.7 20.6 %all-to-all-done = bf16[8,256,512]{1,2,0:T(8,128)(2,1)S(1)} async-done(((bf16[8,256,512]{1,2,0:T(8,128)(2,1)}), bf16[8,256,512]{1,2,0:T(8,128)(2,1)S(1)}, u32[]{:S(2)}, u32[]{:S(2)}) %all-to-all-start) | async-done | bytes 2097184 | tf_op jit(solution)/shard_map/all_to_all | solution.py:22
  60.9 1.8 fusion.2
  62.6 2.2 fusion.86
  65.5 28.2 %all-gather.2 = f32[16,2,32]{2,1,0:T(2,128)S(1)} all-gather(f32[1,2,32]{2,1,0:T(2,128)S(1)} %bitcast.160), channel_id=2, replica_groups=mesh['sp'=16,'fs'=4,'tp'=8] {'sp'}, dimensions={0}, use_global_device_ids=true | all-gather | bytes 4352 | tf_op jit(solution)/shard_map/all_gather | solution.py:192
  94.0 4.6 %select_exponential_fusion = f32[4,2,64,64,32]{3,4,2,1,0:T(8,128)} fusion(f32[4,2,64,32]{2,3,1,0:T(8,128)S(1)} %copy.67, f32[4,2,64,32]{3,2,1,0:T(8,128)S(1)} %reduce_window_sum.35, pred[64,64]{1,0:T(8,128)(4,1)S(1)} %iota_compare_fusion), kind=kLoop, calls=%fused_computation.5 | loop fusion | flops 2097152 | bytes 4329472 | tf_op jit(solution)/shard_map/exp | solution.py:173
  98.5 11.0 %copy.82 = f32[4,2,64,64,32]{2,3,4,1,0:T(8,128)} copy(f32[4,2,64,64,32]{3,4,2,1,0:T(8,128)} %select_exponential_fusion) | data formatting | bytes 8388608
  109.6 12.5 %all-gather.5.cloned.1.call-done = bf16[4096,896]{1,0:T(8,128)(2,1)} async-done(((bf16[256,896]{1,0:T(8,128)(2,1)}), bf16[4096,896]{1,0:T(8,128)(2,1)}) %all-gather.5.cloned.1.call-update) | async-done | bytes 7340048 | tf_op jit(solution)/shard_map/all_gather | solution.py:17
  122.1 2.2 fusion.18
  125.3 2.0 fusion.13
  127.4 2.0 fusion.38
  129.4 5.8 %while.13 = (s32[]{:T(128)}, f32[2,32,64]{2,1,0:T(8,128)S(1)}, f32[4,2,32,64]{3,2,1,0:T(8,128)}, f32[4,2,32]{2,1,0:T(2,128)S(1)}, f32[4,2,32,64]{3,2,1,0:T(8,128)}, /*index=5*/s32[]{:T(128)}, s32[]{:T(128)}) while((s32[]{:T(128)}, f32[2,32,64]{2,1,0:T(8,128)S(1)}, f32[4,2,32,64]{3,2,1,0:T(8,128)}, f32[4,2,32]{2,1,0:T(2,128)S(1)}, ...), condition=%wide.region_9.10_spmd.clone, body=%wide.region_8.9_spmd.clone.sunk | while | flops 16387 | bytes 99680 | solution.py:188
  135.2 25.9 %all-gather.1 = f32[32,32,64]{2,1,0:T(8,128)} all-gather(f32[2,32,64]{2,1,0:T(8,128)S(1)} %get-tuple-element.33), channel_id=3, replica_groups=mesh['sp'=16,'fs'=4,'tp'=8] {'sp'}, dimensions={0}, use_global_device_ids=true | all-gather | bytes 278528 | tf_op jit(solution)/shard_map/all_gather | solution.py:198
  164.5 5.3 %fusion = f32[4,2,64,64]{2,3,1,0:T(8,128)S(1)} fusion(f32[4,2,64,64,32]{2,3,4,1,0:T(8,128)} %copy.82, f32[4,2,32,64]{3,2,1,0:T(8,128)S(1)} %copy.69, f32[4,2,32,64]{3,2,1,0:T(8,128)} %copy.68), kind=kLoop, calls=%fused_computation.4 | loop fusion | flops 3112960 | bytes 4456448 | tf_op jit(solution)/shard_map/nhid,nhjd,nhijd->nhij/dot_general | solution.py:174
  170.4 2.0 fusion.12
  172.4 2.0 fusion.6
  174.4 2.2 collective-permute-start
  180.4 12.4 %all-to-all-start.1 = ((f32[8,1,512]{2,1,0:T(1,128)}), f32[8,1,512]{2,1,0:T(1,128)S(1)}, u32[]{:S(2)}, u32[]{:S(2)}) async-start(f32[8,1,512]{2,1,0:T(1,128)} %broadcast_in_dim.46), calls=%async_computation.1 | async-start | bytes 32768 | tf_op jit(solution)/shard_map/all_to_all | solution.py:22
  194.0 3.6 %all-to-all-done.1 = f32[8,1,512]{2,1,0:T(1,128)S(1)} async-done(((f32[8,1,512]{2,1,0:T(1,128)}), f32[8,1,512]{2,1,0:T(1,128)S(1)}, u32[]{:S(2)}, u32[]{:S(2)}) %all-to-all-start.1) | async-done | bytes 16416 | tf_op jit(solution)/shard_map/all_to_all | solution.py:22
  197.6 4.1 %fusion.31 = f32[4096,256]{1,0:T(8,128)} fusion(bf16[4096,896]{1,0:T(8,128)(2,1)} %all-gather.5.cloned.1.call-done, f32[256,128]{1,0:T(8,128)} %get-tuple-element.65, f32[128]{0:T(128)} %dynamic_slice.28, f32[256]{0:T(256)S(1)} %get-tuple-element.100, f32[256]{0:T(256)S(1)} %get-tuple-element.99), kind=kOutput, calls=%fused_computation.50 | convolution fusion | flops 268697600 | bytes 5376512 | tf_op jit(solution)/shard_map/dot_general | solution.py:222
  201.7 5.7 %fusion.1 = bf16[4096,256]{1,0:T(8,128)(2,1)} fusion(f32[4096,256]{1,0:T(8,128)} %fusion.31, bf16[4096,896]{1,0:T(8,128)(2,1)} %all-gather.5.cloned.1.call-done, f32[256,128]{1,0:T(8,128)S(1)} %reshape.78, bf16[256,4096]{0,1:T(8,128)(2,1)S(1)} %copy-done.1, f32[256]{0:T(256)S(1)} %add_rsqrt_fusion.1), kind=kOutput, calls=%fused_computation.7 | convolution fusion | flops 539262976 | bytes 10617856 | tf_op jit(solution)/shard_map/dot_general | solution.py:228
  207.3 30.4 %all_to_all.16 = bf16[8,512,256]{2,1,0:T(8,128)(2,1)S(1)} all-to-all(bf16[8,512,256]{2,1,0:T(8,128)(2,1)} %bitcast.150), channel_id=1, replica_groups=mesh['sp'=16,'fs'=4,'tp'=8] {'tp'}, dimensions={0} | all-to-all | bytes 4194304 | tf_op jit(solution)/shard_map/all_to_all | solution.py:66
  (136 shorter events, 25.2 us)
Async XLA Ops:
  6.5 56.1 %copy-start = (bf16[4096,64]{0,1:T(8,128)(2,1)S(1)}, bf16[4096,64]{0,1:T(8,128)(2,1)}, u32[]{:S(2)}) copy-start(bf16[4096,64]{0,1:T(8,128)(2,1)} %param.29) | copy-start | bytes 1572868
  6.5 115.5 %all-gather.5.cloned.1.call-start = ((), (), s32[]{:S(2)}) async-start(), calls=%async_computation.3 | async-start | bytes 7798784 | tf_op jit(solution)/shard_map/all_gather | solution.py:17
  20.9 39.9 %copy-start.6 = (f32[4096]{0:T(1024)S(1)}, f32[4096]{0:T(1024)}, u32[]{:S(2)}) copy-start(f32[4096]{0:T(1024)} %param.20) | copy-start | bytes 49156
  22.4 37.8 %all-to-all-start = ((bf16[8,256,512]{1,2,0:T(8,128)(2,1)}), bf16[8,256,512]{1,2,0:T(8,128)(2,1)S(1)}, u32[]{:S(2)}, u32[]{:S(2)}) async-start(bf16[8,256,512]{1,2,0:T(8,128)(2,1)} %broadcast_in_dim.45), calls=%async_computation | async-start | bytes 4194304 | tf_op jit(solution)/shard_map/all_to_all | solution.py:22
  34.0 28.6 %copy-start.5 = (f32[1,256,64]{1,2,0:T(8,128)S(1)}, f32[1,256,64]{1,2,0:T(8,128)}, u32[]{:S(2)}) copy-start(f32[1,256,64]{1,2,0:T(8,128)} %param.32) | copy-start | bytes 196612
  98.5 23.5 %copy-start.1 = (bf16[256,4096]{0,1:T(8,128)(2,1)S(1)}, bf16[256,4096]{0,1:T(8,128)(2,1)}, u32[]{:S(2)}) copy-start(bf16[256,4096]{0,1:T(8,128)(2,1)} %fusion.2) | copy-start | bytes 6291460
  170.1 8.2 %copy-start.7 = (f32[128]{0:T(128)S(1)}, f32[128]{0:T(128)}, u32[]{:S(2)}) copy-start(f32[128]{0:T(128)} %get-tuple-element.69) | copy-start | bytes 1540
  170.1 8.2 %copy-start.8 = (f32[128]{0:T(128)S(1)}, f32[128]{0:T(128)}, u32[]{:S(2)}) copy-start(f32[128]{0:T(128)} %get-tuple-element.70) | copy-start | bytes 1540
  170.1 8.2 %copy-start.9 = (f32[128]{0:T(128)S(1)}, f32[128]{0:T(128)}, u32[]{:S(2)}) copy-start(f32[128]{0:T(128)} %get-tuple-element.71) | copy-start | bytes 1540
  170.2 8.2 %copy-start.10 = (f32[128]{0:T(128)S(1)}, f32[128]{0:T(128)}, u32[]{:S(2)}) copy-start(f32[128]{0:T(128)} %get-tuple-element.72) | copy-start | bytes 1540
  170.2 8.2 %copy-start.11 = (f32[128]{0:T(128)S(1)}, f32[128]{0:T(128)}, u32[]{:S(2)}) copy-start(f32[128]{0:T(128)} %get-tuple-element.73) | copy-start | bytes 1540
  170.2 8.2 %copy-start.12 = (f32[128]{0:T(128)S(1)}, f32[128]{0:T(128)}, u32[]{:S(2)}) copy-start(f32[128]{0:T(128)} %get-tuple-element.74) | copy-start | bytes 1540
  170.2 8.2 %copy-start.13 = (f32[128]{0:T(128)S(1)}, f32[128]{0:T(128)}, u32[]{:S(2)}) copy-start(f32[128]{0:T(128)} %get-tuple-element.75) | copy-start | bytes 1540
  170.2 8.2 %copy-start.14 = (f32[128]{0:T(128)S(1)}, f32[128]{0:T(128)}, u32[]{:S(2)}) copy-start(f32[128]{0:T(128)} %get-tuple-element.76) | copy-start | bytes 1540
  170.2 8.2 %copy-start.15 = (f32[128]{0:T(128)S(1)}, f32[128]{0:T(128)}, u32[]{:S(2)}) copy-start(f32[128]{0:T(128)} %get-tuple-element.77) | copy-start | bytes 1540
  170.2 8.2 %copy-start.16 = (f32[128]{0:T(128)S(1)}, f32[128]{0:T(128)}, u32[]{:S(2)}) copy-start(f32[128]{0:T(128)} %get-tuple-element.78) | copy-start | bytes 1540
  170.2 8.2 %copy-start.17 = (f32[128]{0:T(128)S(1)}, f32[128]{0:T(128)}, u32[]{:S(2)}) copy-start(f32[128]{0:T(128)} %get-tuple-element.79) | copy-start | bytes 1540
  170.2 8.2 %copy-start.18 = (f32[128]{0:T(128)S(1)}, f32[128]{0:T(128)}, u32[]{:S(2)}) copy-start(f32[128]{0:T(128)} %get-tuple-element.80) | copy-start | bytes 1540
  170.2 8.2 %copy-start.19 = (f32[128]{0:T(128)S(1)}, f32[128]{0:T(128)}, u32[]{:S(2)}) copy-start(f32[128]{0:T(128)} %get-tuple-element.81) | copy-start | bytes 1540
  170.3 8.2 %copy-start.20 = (f32[128]{0:T(128)S(1)}, f32[128]{0:T(128)}, u32[]{:S(2)}) copy-start(f32[128]{0:T(128)} %get-tuple-element.82) | copy-start | bytes 1540
  170.3 8.2 %copy-start.21 = (f32[128]{0:T(128)S(1)}, f32[128]{0:T(128)}, u32[]{:S(2)}) copy-start(f32[128]{0:T(128)} %get-tuple-element.83) | copy-start | bytes 1540
  170.3 8.2 %copy-start.22 = (f32[128]{0:T(128)S(1)}, f32[128]{0:T(128)}, u32[]{:S(2)}) copy-start(f32[128]{0:T(128)} %get-tuple-element.84) | copy-start | bytes 1540
  174.4 3.9 %collective-permute-start = (bf16[30,128]{1,0:T(8,128)(2,1)S(1)}, bf16[30,128]{1,0:T(8,128)(2,1)S(1)}, u32[]{:S(2)}, u32[]{:S(2)}) collective-permute-start(bf16[30,128]{1,0:T(8,128)(2,1)S(1)} %slice.265), channel_id=1, source_target_pairs={{0,32},{32,64},{64,96},{96,128},{128,160},{160,192},{192,224},{224... | collective-permute-start | bytes 23048 | tf_op jit(solution)/shard_map/ppermute | solution.py:41
  180.4 17.1 %all-to-all-start.1 = ((f32[8,1,512]{2,1,0:T(1,128)}), f32[8,1,512]{2,1,0:T(1,128)S(1)}, u32[]{:S(2)}, u32[]{:S(2)}) async-start(f32[8,1,512]{2,1,0:T(1,128)} %broadcast_in_dim.46), calls=%async_computation.1 | async-start | bytes 32768 | tf_op jit(solution)/shard_map/all_to_all | solution.py:22
  (17 other events, 137.1 us)
Sparse Core Ops, SparseCore 0:
  20.0 102.0 all-gather.4
where the time goes:
time: 247 us; the launch traced here: 246 us
  blocking collectives  96.8 us (39%)
  waiting for transfers between devices  36.6 us (15%)
  starting transfers between devices  26.3 us (11%)
  matrix products  25.9 us (10%)
  local copies, waits for them, and re-layouts  25.3 us (10%)
  other arithmetic  20.7 us (8%)
  between operations  14.1 us (6%)
    all_to_all x1, blocking collectives, sum_at_owner(): lax.all_to_all(in_blocks(value, dim, length), axis, 0, 0, tiled=True)  30.4 us
    all_gather x1, blocking collectives, shards(): totals = lax.all_gather(device_total[None], 'sp', axis=0, tiled=True)  28.2 us
    all_gather x1, blocking collectives, shards(): piece = lax.all_gather(local_final[None], 'sp', axis=0, tiled=True)  25.9 us
    all_to_all x2, waiting for transfers between devices, from_everyone(): lax.all_to_all(jnp.broadcast_to(value[None], (length, *value.shape)), axi...  24.1 us
    all_to_all x2, starting transfers between devices, from_everyone(): lax.all_to_all(jnp.broadcast_to(value[None], (length, *value.shape)), axi...  24 us
    all_gather x1, waiting for transfers between devices, side_by_side(): lax.all_gather(both, axis, axis=dim, tiled=True)  12.5 us
    all_gather x1, blocking collectives, side_by_side(): lax.all_gather(both, axis, axis=dim, tiled=True)  12.3 us
    unnamed x76, local copies, waits for them, and re-layouts  12.3 us
  transfers between devices with their start and end apart: 4, of which 3 were waited for; matrix products, arithmetic and copies ran while one was open for 13% of the time, Pallas kernels for 0%

commit v1 on v0

--- a/solution.py
+++ b/solution.py
@@ -195,7 +195,10 @@
     before = lax.dynamic_index_in_dim(
         running_totals, sp_index, 0, False
     ) - lax.dynamic_index_in_dim(totals, sp_index, 0, False)
-    piece = lax.all_gather(local_final[None], "sp", axis=0, tiled=True)
+    report_bars = lambda chunk: jnp.concatenate(
+        lax.all_to_all(jnp.stack([chunk] * lax.axis_size("sp")), "sp", 0, 0), axis=0
+    )
+    piece = report_bars(local_final[None])
     number = piece.shape[0]
     anchor = jnp.arange(number, dtype=jnp.int32)
     exponent = jnp.where(

time: 247 us -> 238 us (0.964)
  blocking collectives: 96.8 us -> 75.9 us
  local copies, waits for them, and re-layouts: 25.3 us -> 31 us
  other arithmetic: 20.7 us -> 24.4 us
  matrix products: 25.9 us -> 28.6 us
  waiting for transfers between devices: 36.6 us -> 33.9 us
    all_gather x1 -> x0, blocking collectives: 25.9 us -> none  [shards(): piece = lax.all_gather(local_final[None], 'sp', axis=0, tiled=True)]
    all_to_all x0 -> x1, starting transfers between devices: none -> 10.2 us  [shards(): lax.all_to_all(jnp.stack([chunk] * lax.axis_size('sp')), 'sp', 0, 0)]
    all_to_all x2, starting transfers between devices: 24 us -> 17.2 us  [from_everyone(): lax.all_to_all(jnp.broadcast_to(value[None], (length, *value.shape)), axi...]
    all_to_all x1, blocking collectives: 30.4 us -> 35.4 us  [sum_at_owner(): lax.all_to_all(in_blocks(value, dim, length), axis, 0, 0, tiled=True)]
    all_to_all x2, waiting for transfers between devices: 24.1 us -> 20.5 us  [from_everyone(): lax.all_to_all(jnp.broadcast_to(value[None], (length, *value.shape)), axi...]
    unnamed x76 -> x24, local copies, waits for them, and re-layouts: 12.3 us -> 15.2 us
  transfers between devices with their start and end apart: 4 -> 5, of which waited for: 3 -> 3; matrix products, arithmetic and copies ran while one was open for 13% -> 24% of each run, Pallas kernels for 0% -> 0%
where the time goes in v1:
time: 238 us; the launch traced here: 236 us
  blocking collectives  75.9 us (32%)
  waiting for transfers between devices  33.9 us (14%)
  local copies, waits for them, and re-layouts  31 us (13%)
  starting transfers between devices  28.6 us (12%)
  matrix products  28.6 us (12%)
  other arithmetic  24.4 us (10%)
  between operations  13.7 us (6%)
    all_to_all x1, blocking collectives, sum_at_owner(): lax.all_to_all(in_blocks(value, dim, length), axis, 0, 0, tiled=True)  35.4 us
    all_gather x1, blocking collectives, shards(): totals = lax.all_gather(device_total[None], 'sp', axis=0, tiled=True)  28.2 us
    all_to_all x2, waiting for transfers between devices, from_everyone(): lax.all_to_all(jnp.broadcast_to(value[None], (length, *value.shape)), axi...  20.5 us
    all_to_all x2, starting transfers between devices, from_everyone(): lax.all_to_all(jnp.broadcast_to(value[None], (length, *value.shape)), axi...  17.2 us
    unnamed x24, local copies, waits for them, and re-layouts  15.2 us
    all_gather x1, blocking collectives, side_by_side(): lax.all_gather(both, axis, axis=dim, tiled=True)  12.3 us
    all_gather x1, waiting for transfers between devices, side_by_side(): lax.all_gather(both, axis, axis=dim, tiled=True)  12 us
    all_to_all x1, starting transfers between devices, shards(): lax.all_to_all(jnp.stack([chunk] * lax.axis_size('sp')), 'sp', 0, 0)  10.2 us
  transfers between devices with their start and end apart: 5, of which 3 were waited for; matrix products, arithmetic and copies ran while one was open for 24% of the time, Pallas kernels for 0%

profile of v1, /device:TPU:1, one launch (start us, length us, event | category | flops | bytes accessed | tf_op | source)
XLA Modules:
  0.0 236.2 jit_solution(380675715664380731)
XLA Ops:
  7.5 12.3 %all_gather.9 = bf16[256,896]{1,0:T(8,128)(2,1)} all-gather(bf16[64,896]{1,0:T(8,128)(2,1)S(1)} %concatenate.11), channel_id=1, replica_groups=mesh['sp'=16,'fs'=4,'tp'=8] {'fs'}, dimensions={0}, use_global_device_ids=true | all-gather | bytes 573440 | tf_op jit(solution)/shard_map/all_gather | solution.py:17
  22.4 11.6 %all-to-all-start = ((bf16[8,256,512]{1,2,0:T(8,128)(2,1)}), bf16[8,256,512]{1,2,0:T(8,128)(2,1)S(1)}, u32[]{:S(2)}, u32[]{:S(2)}) async-start(bf16[8,256,512]{1,2,0:T(8,128)(2,1)} %broadcast_in_dim.39), calls=%async_computation | async-start | bytes 4194304 | tf_op jit(solution)/shard_map/all_to_all | solution.py:22
  37.8 2.0 fusion.98
  39.8 20.5 %all-to-all-done = bf16[8,256,512]{1,2,0:T(8,128)(2,1)S(1)} async-done(((bf16[8,256,512]{1,2,0:T(8,128)(2,1)}), bf16[8,256,512]{1,2,0:T(8,128)(2,1)S(1)}, u32[]{:S(2)}, u32[]{:S(2)}) %all-to-all-start) | async-done | bytes 2097184 | tf_op jit(solution)/shard_map/all_to_all | solution.py:22
  62.7 2.2 fusion.86
  65.6 28.2 %all-gather.1 = f32[16,2,32]{2,1,0:T(2,128)S(1)} all-gather(f32[1,2,32]{2,1,0:T(2,128)S(1)} %bitcast.160), channel_id=2, replica_groups=mesh['sp'=16,'fs'=4,'tp'=8] {'sp'}, dimensions={0}, use_global_device_ids=true | all-gather | bytes 4352 | tf_op jit(solution)/shard_map/all_gather | solution.py:192
  94.0 4.5 %select_exponential_fusion = f32[4,2,64,64,32]{3,4,2,1,0:T(8,128)} fusion(f32[4,2,64,32]{2,3,1,0:T(8,128)S(1)} %copy.67, f32[4,2,64,32]{3,2,1,0:T(8,128)S(1)} %reduce_window_sum.35, pred[64,64]{1,0:T(8,128)(4,1)S(1)} %iota_compare_fusion), kind=kLoop, calls=%fused_computation.5 | loop fusion | flops 2097152 | bytes 4329472 | tf_op jit(solution)/shard_map/exp | solution.py:173
  98.5 11.0 %copy.82 = f32[4,2,64,64,32]{2,3,4,1,0:T(8,128)} copy(f32[4,2,64,64,32]{3,4,2,1,0:T(8,128)} %select_exponential_fusion) | data formatting | bytes 8388608
  110.1 12.0 %all-gather.4.cloned.1.call-done = bf16[4096,896]{1,0:T(8,128)(2,1)} async-done(((bf16[256,896]{1,0:T(8,128)(2,1)}), bf16[4096,896]{1,0:T(8,128)(2,1)}) %all-gather.4.cloned.1.call-update) | async-done | bytes 7340048 | tf_op jit(solution)/shard_map/all_gather | solution.py:17
  122.1 2.2 fusion.18
  125.3 2.0 fusion.13
  127.4 2.0 fusion.12
  129.4 2.0 fusion.6
  134.3 5.8 %while.13 = (s32[]{:T(128)}, f32[2,32,64]{2,1,0:T(8,128)S(1)}, f32[4,2,32,64]{3,2,1,0:T(8,128)}, f32[4,2,32]{2,1,0:T(2,128)S(1)}, f32[4,2,32,64]{3,2,1,0:T(8,128)}, /*index=5*/s32[]{:T(128)}, s32[]{:T(128)}) while((s32[]{:T(128)}, f32[2,32,64]{2,1,0:T(8,128)S(1)}, f32[4,2,32,64]{3,2,1,0:T(8,128)}, f32[4,2,32]{2,1,0:T(2,128)S(1)}, ...), condition=%wide.region_9.10_spmd.clone, body=%wide.region_8.9_spmd.clone.sunk | while | flops 16387 | bytes 99680 | solution.py:188
  140.2 2.0 fusion.101
  142.8 5.6 %all-to-all-start.1 = ((f32[8,1,512]{2,1,0:T(1,128)}), f32[8,1,512]{2,1,0:T(1,128)S(1)}, u32[]{:S(2)}, u32[]{:S(2)}) async-start(f32[8,1,512]{2,1,0:T(1,128)} %broadcast_in_dim.44), calls=%async_computation.1 | async-start | bytes 32768 | tf_op jit(solution)/shard_map/all_to_all | solution.py:22
  151.0 2.1 reshape.98
  154.6 10.2 %all-to-all-start.2 = ((f32[16,1,4096]{2,1,0:T(1,128)}), f32[16,1,4096]{2,1,0:T(1,128)}, u32[]{:S(2)}, u32[]{:S(2)}) async-start(f32[16,1,4096]{2,1,0:T(1,128)} %reshape.98), calls=%async_computation.2 | async-start | bytes 524288 | tf_op jit(solution)/shard_map/all_to_all | solution.py:199
  164.7 6.0 %fusion = f32[4,2,64,64]{2,3,1,0:T(8,128)} fusion(f32[4,2,64,64,32]{2,3,4,1,0:T(8,128)} %copy.82, f32[4,2,32,64]{3,2,1,0:T(8,128)} %copy.69, f32[4,2,32,64]{3,2,1,0:T(8,128)} %copy.68), kind=kLoop, calls=%fused_computation.4 | loop fusion | flops 3112960 | bytes 4456448 | tf_op jit(solution)/shard_map/nhid,nhjd,nhijd->nhij/dot_general | solution.py:174
  171.6 2.0 fusion.73
  173.7 4.0 %fusion.31 = f32[4096,256]{1,0:T(8,128)} fusion(bf16[4096,896]{1,0:T(8,128)(2,1)} %all-gather.4.cloned.1.call-done, f32[256,128]{1,0:T(8,128)} %get-tuple-element.65, f32[128]{0:T(128)S(1)} %copy-done.9, f32[256]{0:T(256)S(1)} %get-tuple-element.100, f32[256]{0:T(256)S(1)} %get-tuple-element.99), kind=kOutput, calls=%fused_computation.50 | convolution fusion | flops 268697600 | bytes 5376512 | tf_op jit(solution)/shard_map/dot_general | solution.py:225
  179.6 2.2 reduce.6
  187.1 5.7 %fusion.1 = bf16[4096,256]{1,0:T(8,128)(2,1)} fusion(f32[4096,256]{1,0:T(8,128)} %fusion.31, bf16[4096,896]{1,0:T(8,128)(2,1)} %all-gather.4.cloned.1.call-done, f32[256,128]{1,0:T(8,128)S(1)} %reshape.84, bf16[256,4096]{0,1:T(8,128)(2,1)S(1)} %copy-done.1, f32[256]{0:T(256)S(1)} %copy-done.7), kind=kOutput, calls=%fused_computation.7 | convolution fusion | flops 539262976 | bytes 10617856 | tf_op jit(solution)/shard_map/dot_general | solution.py:231
  192.8 35.4 %all_to_all.21 = bf16[8,512,256]{2,1,0:T(8,128)(2,1)S(1)} all-to-all(bf16[8,512,256]{2,1,0:T(8,128)(2,1)} %bitcast.150), channel_id=1, replica_groups=mesh['sp'=16,'fs'=4,'tp'=8] {'tp'}, dimensions={0} | all-to-all | bytes 4194304 | tf_op jit(solution)/shard_map/all_to_all | solution.py:66
  (88 shorter events, 35.0 us)
Async XLA Ops:
  6.5 56.1 %copy-start = (bf16[4096,64]{0,1:T(8,128)(2,1)S(1)}, bf16[4096,64]{0,1:T(8,128)(2,1)}, u32[]{:S(2)}) copy-start(bf16[4096,64]{0,1:T(8,128)(2,1)} %param.29) | copy-start | bytes 1572868
  6.5 115.5 %all-gather.4.cloned.1.call-start = ((), (), s32[]{:S(2)}) async-start(), calls=%async_computation.4 | async-start | bytes 7798784 | tf_op jit(solution)/shard_map/all_gather | solution.py:17
  20.9 39.9 %copy-start.4 = (f32[4096]{0:T(1024)S(1)}, f32[4096]{0:T(1024)}, u32[]{:S(2)}) copy-start(f32[4096]{0:T(1024)} %param.20) | copy-start | bytes 49156
  22.4 37.8 %all-to-all-start = ((bf16[8,256,512]{1,2,0:T(8,128)(2,1)}), bf16[8,256,512]{1,2,0:T(8,128)(2,1)S(1)}, u32[]{:S(2)}, u32[]{:S(2)}) async-start(bf16[8,256,512]{1,2,0:T(8,128)(2,1)} %broadcast_in_dim.39), calls=%async_computation | async-start | bytes 4194304 | tf_op jit(solution)/shard_map/all_to_all | solution.py:22
  34.0 28.6 %copy-start.3 = (f32[1,256,64]{1,2,0:T(8,128)S(1)}, f32[1,256,64]{1,2,0:T(8,128)}, u32[]{:S(2)}) copy-start(f32[1,256,64]{1,2,0:T(8,128)} %param.32) | copy-start | bytes 196612
  60.9 68.5 %copy-start.6 = (f32[256]{0:T(256)}, f32[256]{0:T(256)S(1)}, u32[]{:S(2)}) copy-start(f32[256]{0:T(256)S(1)} %add_rsqrt_fusion.1) | copy-start | bytes 3076
  98.5 23.6 %copy-start.1 = (bf16[256,4096]{0,1:T(8,128)(2,1)S(1)}, bf16[256,4096]{0,1:T(8,128)(2,1)}, u32[]{:S(2)}) copy-start(bf16[256,4096]{0,1:T(8,128)(2,1)} %fusion.2) | copy-start | bytes 6291460
  127.4 5.9 %copy-start.2 = (f32[4,64,2,32]{3,1,2,0:T(8,128)S(1)}, f32[4,64,2,32]{3,1,2,0:T(8,128)}, u32[]{:S(2)}) copy-start(f32[4,64,2,32]{3,1,2,0:T(8,128)} %copy.73) | copy-start | bytes 196612
  132.0 8.2 %collective-permute-start = (bf16[30,128]{1,0:T(8,128)(2,1)}, bf16[30,128]{1,0:T(8,128)(2,1)S(1)}, u32[]{:S(2)}, u32[]{:S(2)}) collective-permute-start(bf16[30,128]{1,0:T(8,128)(2,1)} %slice.265), channel_id=1, source_target_pairs={{0,32},{32,64},{64,96},{96,128},{128,160},{160,192},{192,224},{224... | collective-permute-start | bytes 23048 | tf_op jit(solution)/shard_map/ppermute | solution.py:41
  142.8 11.8 %all-to-all-start.1 = ((f32[8,1,512]{2,1,0:T(1,128)}), f32[8,1,512]{2,1,0:T(1,128)S(1)}, u32[]{:S(2)}, u32[]{:S(2)}) async-start(f32[8,1,512]{2,1,0:T(1,128)} %broadcast_in_dim.44), calls=%async_computation.1 | async-start | bytes 32768 | tf_op jit(solution)/shard_map/all_to_all | solution.py:22
  154.6 24.6 %all-to-all-start.2 = ((f32[16,1,4096]{2,1,0:T(1,128)}), f32[16,1,4096]{2,1,0:T(1,128)}, u32[]{:S(2)}, u32[]{:S(2)}) async-start(f32[16,1,4096]{2,1,0:T(1,128)} %reshape.98), calls=%async_computation.2 | async-start | bytes 524288 | tf_op jit(solution)/shard_map/all_to_all | solution.py:199
  164.7 8.9 %copy-start.9 = (f32[128]{0:T(128)S(1)}, f32[128]{0:T(128)}, u32[]{:S(2)}) copy-start(f32[128]{0:T(128)} %dynamic_slice.28) | copy-start | bytes 1540
  170.7 14.0 %copy-start.5 = (f32[4,2,32]{2,1,0:T(2,128)S(1)}, f32[4,2,32]{2,1,0:T(2,128)}, u32[]{:S(2)}) copy-start(f32[4,2,32]{2,1,0:T(2,128)} %fusion.23) | copy-start | bytes 3076
  173.6 13.0 %copy-start.8 = (f32[64]{0:T(128)S(1)}, f32[64]{0:T(128)}, u32[]{:S(2)}) copy-start(f32[64]{0:T(128)} %param.35) | copy-start | bytes 772
  173.6 13.5 %copy-start.7 = (f32[256]{0:T(256)S(1)}, f32[256]{0:T(256)}, u32[]{:S(2)}) copy-start(f32[256]{0:T(256)} %copy-done.6) | copy-start | bytes 3076
Sparse Core Ops, SparseCore 0:
  20.0 102.0 all-gather.3
